TPU v7x, 32 devices: a whole 2x2x4 slice. The times are simulated.
32 devices in a mesh: sp: 8 (over z, x), tp: 4 (over y, core).
Axes of the slice: x: 2, y: 2, z: 4, core: 2. Of those that a mesh axis runs over, the one named last changes fastest.
Arguments:
- residual: bfloat16 [2048, 2048], P('sp', 'tp'), may hold values from -8 to 8
- query_latent: bfloat16 [2048, 512], P('sp'), may hold values from -6 to 6
- shared_latent: bfloat16 [2048, 256], P('sp'), may hold values from -6 to 6
- rotary_key: bfloat16 [2048, 32], P('sp'), may hold values from -300 to 300
- query_gain: float32 [512], replicated, may hold values from 0.1 to 1.9
- latent_gain: float32 [256], replicated, may hold values from 0.1 to 1.9
- query_narrow: bfloat16 [512, 384], P(None, 'tp'), may hold values from -0.5 to 0.5
- key_narrow: bfloat16 [256, 256], P(None, 'tp'), may hold values from -0.375 to 0.375
- value_narrow: bfloat16 [256, 256], P(None, 'tp'), may hold values from -0.375 to 0.375
- query_wide: bfloat16 [512, 640], P(None, 'tp'), may hold values from -0.5 to 0.5
- key_wide: bfloat16 [256, 512], P(None, 'tp'), may hold values from -0.375 to 0.375
- value_wide: bfloat16 [256, 512], P(None, 'tp'), may hold values from -0.375 to 0.375
- output_narrow: bfloat16 [256, 2048], P('tp'), may hold values from -1.75 to 1.75
- output_wide: bfloat16 [512, 2048], P('tp'), may hold values from -1.75 to 1.75
- first_gain: float32 [2048], P('tp'), may hold values from 0.1 to 1.9
- first_bias: float32 [2048], P('tp'), may hold values from -1.5 to 1.5
- gate_weight: bfloat16 [2048, 5632], P('sp', 'tp'), may hold values from -0.125 to 0.125
- up_weight: bfloat16 [2048, 5632], P('sp', 'tp'), may hold values from -0.125 to 0.125
- down_weight: bfloat16 [5632, 2048], P('tp', 'sp'), may hold values from -0.078125 to 0.078125
- second_gain: float32 [2048], P('tp'), may hold values from 0.1 to 1.9
- second_bias: float32 [2048], P('tp'), may hold values from -1.5 to 1.5
Outputs:
- layer_out: bfloat16 [2048, 2048], P('sp', 'tp')
All inputs are finite; a program needn't handle non-finite values.
Results may differ from a plain program's by a relative error of at most 0.017.
The roundings to bfloat16 on the way count: a program that leaves them out, or rounds other values in their place, can miss the bound.
Values may be sent and summed in bfloat16 or wider, within the bound.
No kernel may reach another device: no remote copies, remote signals or barrier semaphores. Data moves between devices by JAX's collectives and lax.ppermute only.
A program may use at most 192 MiB of HBM per device.

v0:
```python
import jax
import jax.numpy as jnp
from jax import lax
from jax.sharding import PartitionSpec as P

ROPE = 32
NOPE_A = 64
V_A = 64
NOPE_B = 128
V_B = 128
GRID_W = 64
EPS_ROOT = 1e-06
EPS_LAYER = 1e-05
THETA = 10000.0
DEEP_ALPHA = 2.0**0.25


def rotate(half_part, angle):
    lower, upper = jnp.split(half_part, 2, axis=-1)
    cosine = jnp.cos(angle)
    sine = jnp.sin(angle)
    return jnp.concatenate([lower * cosine - upper * sine, upper * cosine + lower * sine], axis=-1)


def turn_axial(values_in, positions):
    quarter = values_in.shape[-1] // 4
    freqs = THETA ** (-(2.0 * jnp.arange(quarter, dtype=jnp.float32)) / (2 * quarter))
    row_angle = (positions // GRID_W).astype(jnp.float32)[:, None, None] * freqs
    col_angle = (positions % GRID_W).astype(jnp.float32)[:, None, None] * freqs
    first_half, second_half = jnp.split(values_in, 2, axis=-1)
    return jnp.concatenate([rotate(first_half, row_angle), rotate(second_half, col_angle)], axis=-1)


def root_scale(latent, gain):
    floated = latent.astype(jnp.float32)
    return (
        floated * lax.rsqrt(jnp.mean(floated * floated, axis=-1, keepdims=True) + EPS_ROOT) * gain
    )


def make_query(normed, weight, plain_dim, positions):
    product = jnp.dot(normed, weight, preferred_element_type=jnp.float32)
    head_count = weight.shape[1] // (plain_dim + ROPE)
    product = product.reshape(product.shape[0], head_count, plain_dim + ROPE)
    turned = turn_axial(product[:, :, plain_dim:], positions)
    return jnp.concatenate([product[:, :, :plain_dim], turned], axis=-1).astype(jnp.bfloat16)


def fresh_state(row_count, head_count, value_dim):
    largest = jnp.full((head_count, row_count), -jnp.inf, jnp.float32)
    totals = jnp.zeros((head_count, row_count), jnp.float32)
    weighted = jnp.zeros((row_count, head_count, value_dim), jnp.float32)
    return (largest, totals, weighted)


def update(state_now, queries, key_rows, value_rows, rotary_rows, plain_dim):
    largest, totals, weighted = state_now
    score_scale = queries.shape[2] ** (-0.5)
    scores = jnp.einsum(
        "qhd,khd->hqk", queries[:, :, :plain_dim], key_rows, preferred_element_type=jnp.float32
    )
    scores = scores + jnp.einsum(
        "qhd,kd->hqk", queries[:, :, plain_dim:], rotary_rows, preferred_element_type=jnp.float32
    )
    scores = scores * score_scale
    new_largest = jnp.max(scores, axis=-1)
    factor = jnp.exp(largest - new_largest)
    raised = jnp.exp(scores - new_largest[:, :, None])
    totals = totals * factor + jnp.sum(raised, axis=-1)
    added = jnp.einsum(
        "hqk,khd->qhd", raised.astype(jnp.bfloat16), value_rows, preferred_element_type=jnp.float32
    )
    weighted = weighted * factor.T[:, :, None] + added
    return (new_largest, totals, weighted)


def finish(state_now):
    largest, totals, weighted = state_now
    output = (weighted / totals.T[:, :, None]).astype(jnp.bfloat16)
    return output.reshape(output.shape[0], output.shape[1] * output.shape[2])


def finish_norm(summed, sums, squares, gain, bias, width_total):
    center = sums / width_total
    spread = squares / width_total - center * center
    normed = (summed - center[:, None]) * lax.rsqrt(spread + EPS_LAYER)[:, None]
    return (normed * gain + bias).astype(jnp.bfloat16)


def body(
    residual,
    query_latent,
    shared_latent,
    rotary_key,
    query_gain,
    latent_gain,
    query_narrow,
    key_narrow,
    value_narrow,
    query_wide,
    key_wide,
    value_wide,
    output_narrow,
    output_wide,
    first_gain,
    first_bias,
    gate_weight,
    up_weight,
    down_weight,
    second_gain,
    second_bias,
):
    row_count = residual.shape[0]
    offset = lax.axis_index("sp") * row_count
    positions = offset + jnp.arange(row_count, dtype=jnp.int32)
    query_normed = root_scale(query_latent, query_gain).astype(jnp.bfloat16)
    narrow_queries = make_query(query_normed, query_narrow, NOPE_A, positions)
    wide_queries = make_query(query_normed, query_wide, NOPE_B, positions)
    narrow_heads = narrow_queries.shape[1]
    wide_heads = wide_queries.shape[1]
    start_state = (
        fresh_state(row_count, narrow_heads, V_A),
        fresh_state(row_count, wide_heads, V_B),
    )
    shard_rows = (
        lax.all_gather(shared_latent, "sp", axis=0, tiled=True),
        lax.all_gather(rotary_key, "sp", axis=0, tiled=True),
    )
    latent_rows = shard_rows[0]
    normed = root_scale(latent_rows, latent_gain).astype(jnp.bfloat16)
    count = latent_rows.shape[0]
    narrow_keys = jnp.dot(normed, key_narrow, preferred_element_type=jnp.float32).astype(
        jnp.bfloat16
    )
    narrow_vals = jnp.dot(normed, value_narrow, preferred_element_type=jnp.float32).astype(
        jnp.bfloat16
    )
    wide_keys = jnp.dot(normed, key_wide, preferred_element_type=jnp.float32).astype(jnp.bfloat16)
    wide_vals = jnp.dot(normed, value_wide, preferred_element_type=jnp.float32).astype(jnp.bfloat16)
    key_positions = jnp.arange(count, dtype=jnp.int32)
    rotated = turn_axial(shard_rows[1].astype(jnp.float32)[:, None, :], key_positions)[
        :, 0, :
    ].astype(jnp.bfloat16)
    count = rotated.shape[0]
    narrow_state = update(
        start_state[0],
        narrow_queries,
        narrow_keys.reshape(count, narrow_heads, NOPE_A),
        narrow_vals.reshape(count, narrow_heads, V_A),
        rotated,
        NOPE_A,
    )
    wide_state = update(
        start_state[1],
        wide_queries,
        wide_keys.reshape(count, wide_heads, NOPE_B),
        wide_vals.reshape(count, wide_heads, V_B),
        rotated,
        NOPE_B,
    )
    narrow_out = finish(narrow_state)
    wide_out = finish(wide_state)
    terms = jnp.dot(narrow_out, output_narrow, preferred_element_type=jnp.float32)
    terms = terms + jnp.dot(wide_out, output_wide, preferred_element_type=jnp.float32)
    mixed = lax.psum_scatter(
        terms.astype(jnp.bfloat16), "tp", scatter_dimension=1, tiled=True
    ).astype(jnp.float32)
    width_total = mixed.shape[1] * lax.axis_size("tp")
    summed = DEEP_ALPHA * residual.astype(jnp.float32) + mixed
    sums, squares = lax.psum((jnp.sum(summed, axis=1), jnp.sum(summed * summed, axis=1)), "tp")
    normed_first = finish_norm(summed, sums, squares, first_gain, first_bias, width_total)
    full_rows = lax.all_gather(normed_first, "tp", axis=1, tiled=True)
    shard_rows = (
        lax.all_gather(gate_weight, "sp", axis=0, tiled=True),
        lax.all_gather(up_weight, "sp", axis=0, tiled=True),
    )
    gate_part = jnp.dot(full_rows, shard_rows[0], preferred_element_type=jnp.float32)
    lifted_part = jnp.dot(full_rows, shard_rows[1], preferred_element_type=jnp.float32)
    hidden = (jax.nn.silu(gate_part) * lifted_part).astype(jnp.bfloat16)
    feed_terms = jnp.dot(
        hidden,
        lax.all_gather(down_weight, "sp", axis=1, tiled=True),
        preferred_element_type=jnp.float32,
    )
    feed = lax.psum_scatter(
        feed_terms.astype(jnp.bfloat16), "tp", scatter_dimension=1, tiled=True
    ).astype(jnp.float32)
    summed_two = DEEP_ALPHA * normed_first.astype(jnp.float32) + feed
    sums_two, squares_two = lax.psum(
        (jnp.sum(summed_two, axis=1), jnp.sum(summed_two * summed_two, axis=1)), "tp"
    )
    return finish_norm(summed_two, sums_two, squares_two, second_gain, second_bias, width_total)


def solution(mesh):
    return jax.shard_map(
        body,
        mesh=mesh,
        in_specs=(
            P("sp", "tp"),
            P("sp", None),
            P("sp", None),
            P("sp", None),
            P(),
            P(),
            P(None, "tp"),
            P(None, "tp"),
            P(None, "tp"),
            P(None, "tp"),
            P(None, "tp"),
            P(None, "tp"),
            P("tp", None),
            P("tp", None),
            P("tp"),
            P("tp"),
            P("sp", "tp"),
            P("sp", "tp"),
            P("tp", "sp"),
            P("tp"),
            P("tp"),
        ),
        out_specs=P("sp", "tp"),
        check_vma=False,
    )
```

profile of v0, /device:TPU:0, one launch (start us, length us, event | category | flops | bytes accessed | tf_op | source)
XLA Modules:
  0.0 453.0 jit_solution(9527016040940097273)
XLA Ops:
  6.5 0.7 all-gather.6.cloned.1.call-update
  7.4 32.8 %all_gather.19 = bf16[2048,32]{0,1:T(8,128)(2,1)S(1)} all-gather(bf16[256,32]{0,1:T(8,128)(2,1)} %param.24), channel_id=1, replica_groups=mesh['sp'=8,'tp'=4] {'sp'}, dimensions={0}, use_global_device_ids=true | all-gather | bytes 147456 | tf_op jit(solution)/shard_map/all_gather | solution.py:127
  40.2 1.1 fusion.31
  41.3 1.3 convolution_bitcast_fusion.5
  42.6 1.3 convolution_bitcast_fusion.4
  44.1 0.6 fusion.59
  44.7 7.9 %all-gather.6.cloned.1.call-done = bf16[2048,256]{1,0:T(8,128)(2,1)} async-done(((bf16[256,256]{1,0:T(8,128)(2,1)}), bf16[2048,256]{1,0:T(8,128)(2,1)}) %all-gather.6.cloned.1.call-update) | async-done | bytes 1048592 | tf_op jit(solution)/shard_map/all_gather | solution.py:126
  52.5 1.6 fusion.6
  54.1 2.1 convolution_bitcast_fusion.3
  56.3 0.6 fusion.132
  56.9 1.3 copy-done.2
  58.8 2.2 convolution_bitcast_fusion.1
  61.1 2.1 fusion.131
  63.2 1.3 copy-done.3
  65.0 2.6 fusion.20
  67.6 1.8 fusion.133
  69.4 2.6 fusion.24
  72.1 3.1 fusion.4
  75.2 23.7 %reduce-scatter.3.cloned.1.call-done = bf16[256,512]{1,0:T(8,128)(2,1)} async-done(((bf16[256,2048]{1,0:T(8,128)(2,1)}), bf16[256,512]{1,0:T(8,128)(2,1)}) %reduce-scatter.3.cloned.1.call-update) | async-done | bytes 262160 | tf_op jit(solution)/shard_map/reduce_scatter | solution.py:165
  99.0 1.2 fusion.34
  100.1 5.8 %all-reduce.1 = (f32[256]{0:T(256)S(1)}, f32[256]{0:T(256)S(1)}) all-reduce(f32[256]{0:T(256)S(1)} %get-tuple-element.8, f32[256]{0:T(256)S(1)} %get-tuple-element.7), channel_id=1, replica_groups=mesh['sp'=8,'tp'=4] {'tp'}, use_global_device_ids=true, to_apply=%region_10.11 | all-reduce | flops 512 | bytes 4096 | tf_op jit(solution)/shard_map/psum | solution.py:170
  105.9 1.8 add_convert_fusion.1
  109.7 15.5 %all-gather.8.cloned.1.call-done = bf16[256,2048]{1,0:T(8,128)(2,1)} async-done(((bf16[256,512]{1,0:T(8,128)(2,1)}), bf16[256,2048]{1,0:T(8,128)(2,1)}) %all-gather.8.cloned.1.call-update) | async-done | bytes 1048592 | tf_op jit(solution)/shard_map/all_gather | solution.py:172
  125.2 94.4 %all-gather.10.cloned.1.call-done = bf16[2048,1408]{1,0:T(8,128)(2,1)} async-done(((bf16[256,1408]{1,0:T(8,128)(2,1)}), bf16[2048,1408]{1,0:T(8,128)(2,1)}) %all-gather.10.cloned.1.call-update) | async-done | bytes 5767184 | tf_op jit(solution)/shard_map/all_gather | solution.py:174
  219.6 4.8 %fusion.134 = f32[256,1408]{1,0:T(8,128)S(1)} fusion(bf16[256,2048]{1,0:T(8,128)(2,1)} %all-gather.8.cloned.1.call-done, bf16[2048,1408]{1,0:T(8,128)(2,1)} %all-gather.10.cloned.1.call-done), kind=kOutput, calls=%fused_computation.179 | convolution fusion | flops 1476395008 | bytes 8257536 | tf_op jit(solution)/shard_map/dot_general | solution.py:177
  224.4 87.8 %all-gather.12.cloned.1.call-done = bf16[2048,1408]{1,0:T(8,128)(2,1)} async-done(((bf16[256,1408]{1,0:T(8,128)(2,1)}), bf16[2048,1408]{1,0:T(8,128)(2,1)}) %all-gather.12.cloned.1.call-update) | async-done | bytes 5767184 | tf_op jit(solution)/shard_map/all_gather | solution.py:175
  312.2 93.2 %all-gather.14.cloned.1.call-done = bf16[1408,2048]{1,0:T(8,128)(2,1)} async-done(((bf16[1408,256]{1,0:T(8,128)(2,1)}), bf16[1408,2048]{1,0:T(8,128)(2,1)}) %all-gather.14.cloned.1.call-update) | async-done | bytes 5767184 | tf_op jit(solution)/shard_map/all_gather | solution.py:182
  405.4 8.8 %convolution_convert_fusion = bf16[256,2048]{1,0:T(8,128)(2,1)} fusion(bf16[1408,2048]{1,0:T(8,128)(2,1)} %all-gather.14.cloned.1.call-done, bf16[256,2048]{1,0:T(8,128)(2,1)S(1)} %copy-done.14, bf16[2048,1408]{1,0:T(8,128)(2,1)} %all-gather.12.cloned.1.call-done, f32[256,1408]{1,0:T(8,128)S(1)} %fusion.134), kind=kOutput, calls=%fused_computation.14 | convolution fusion | flops 2955476992 | bytes 15073280 | tf_op jit(solution)/shard_map/dot_general | solution.py:180
  414.2 23.1 %reduce-scatter.5.cloned.1.call-done = bf16[256,512]{1,0:T(8,128)(2,1)} async-done(((bf16[256,2048]{1,0:T(8,128)(2,1)}), bf16[256,512]{1,0:T(8,128)(2,1)}) %reduce-scatter.5.cloned.1.call-update) | async-done | bytes 262160 | tf_op jit(solution)/shard_map/reduce_scatter | solution.py:185
  437.4 1.2 fusion.35
  438.5 5.8 %all-reduce = (f32[256]{0:T(256)S(1)}, f32[256]{0:T(256)S(1)}) all-reduce(f32[256]{0:T(256)S(1)} %get-tuple-element.6, f32[256]{0:T(256)S(1)} %get-tuple-element.5), channel_id=1, replica_groups=mesh['sp'=8,'tp'=4] {'tp'}, use_global_device_ids=true, to_apply=%region_15.16 | all-reduce | flops 512 | bytes 4096 | tf_op jit(solution)/shard_map/psum | solution.py:189
  444.3 1.8 add_convert_fusion
  (58 shorter events, 3.4 us)
Async XLA Ops:
  6.5 61.1 %copy-start = (bf16[128,2048]{1,0:T(8,128)(2,1)S(1)}, bf16[128,2048]{1,0:T(8,128)(2,1)}, u32[]{:S(2)}) copy-start(bf16[128,2048]{1,0:T(8,128)(2,1)} %param.34) | copy-start | bytes 1572868
  6.5 47.6 %copy-start.9 = (f32[256]{0:T(256)S(1)}, f32[256]{0:T(256)}, u32[]{:S(2)}) copy-start(f32[256]{0:T(256)} %param.26) | copy-start | bytes 3076
  6.5 47.6 %copy-start.8 = (bf16[256,64]{0,1:T(8,128)(2,1)S(1)}, bf16[256,64]{0,1:T(8,128)(2,1)}, u32[]{:S(2)}) copy-start(bf16[256,64]{0,1:T(8,128)(2,1)} %param.28) | copy-start | bytes 98308
  6.5 46.0 %all-gather.6.cloned.1.call-start = ((), (), s32[]{:S(2)}) async-start(), calls=%async_computation.2 | async-start | bytes 1179648 | tf_op jit(solution)/shard_map/all_gather | solution.py:126
  7.3 91.7 %reduce-scatter.3.cloned.1.call-start = ((), (), s32[]{:S(2)}) async-start(), calls=%async_computation.3 | async-start | bytes 1310720 | tf_op jit(solution)/shard_map/reduce_scatter | solution.py:165
  56.8 1.3 copy-start.2
  56.9 2.0 copy-start.1
  56.9 2.0 copy-start.7
  63.2 1.3 copy-start.3
  63.2 1.8 copy-start.15
  67.6 1.8 copy-start.16
  69.4 2.6 copy-start.6
  72.1 26.9 %copy-start.5 = (bf16[256,512]{1,0:T(8,128)(2,1)S(1)}, bf16[256,512]{1,0:T(8,128)(2,1)}, u32[]{:S(2)}) copy-start(bf16[256,512]{1,0:T(8,128)(2,1)} %param.21) | copy-start | bytes 786436
  72.1 33.8 %copy-start.10 = (f32[512]{0:T(512)S(1)}, f32[512]{0:T(512)}, u32[]{:S(2)}) copy-start(f32[512]{0:T(512)} %param.36) | copy-start | bytes 6148
  72.1 33.8 %copy-start.11 = (f32[512]{0:T(512)S(1)}, f32[512]{0:T(512)}, u32[]{:S(2)}) copy-start(f32[512]{0:T(512)} %param.35) | copy-start | bytes 6148
  75.2 50.0 %all-gather.8.cloned.1.call-start = ((), (), s32[]{:S(2)}) async-start(), calls=%async_computation.4 | async-start | bytes 1310720 | tf_op jit(solution)/shard_map/all_gather | solution.py:172
  107.7 111.8 %all-gather.10.cloned.1.call-start = ((), (), s32[]{:S(2)}) async-start(), calls=%async_computation.5 | async-start | bytes 6488064 | tf_op jit(solution)/shard_map/all_gather | solution.py:174
  108.3 203.8 %all-gather.12.cloned.1.call-start = ((), (), s32[]{:S(2)}) async-start(), calls=%async_computation.6 | async-start | bytes 6488064 | tf_op jit(solution)/shard_map/all_gather | solution.py:175
  108.9 296.5 %all-gather.14.cloned.1.call-start = ((), (), s32[]{:S(2)}) async-start(), calls=%async_computation.7 | async-start | bytes 6488064 | tf_op jit(solution)/shard_map/all_gather | solution.py:182
  109.5 327.9 %reduce-scatter.5.cloned.1.call-start = ((), (), s32[]{:S(2)}) async-start(), calls=%async_computation.8 | async-start | bytes 1310720 | tf_op jit(solution)/shard_map/reduce_scatter | solution.py:185
  125.2 280.2 %copy-start.14 = (bf16[256,2048]{1,0:T(8,128)(2,1)S(1)}, bf16[256,2048]{1,0:T(8,128)(2,1)}, u32[]{:S(2)}) copy-start(bf16[256,2048]{1,0:T(8,128)(2,1)} %all-gather.8.cloned.1.call-done) | copy-start | bytes 3145732
  224.4 213.0 %copy-start.4 = (bf16[256,512]{1,0:T(8,128)(2,1)S(1)}, bf16[256,512]{1,0:T(8,128)(2,1)}, u32[]{:S(2)}) copy-start(bf16[256,512]{1,0:T(8,128)(2,1)} %add_convert_fusion.1) | copy-start | bytes 786436
  224.4 219.9 %copy-start.12 = (f32[512]{0:T(512)S(1)}, f32[512]{0:T(512)}, u32[]{:S(2)}) copy-start(f32[512]{0:T(512)} %param.41) | copy-start | bytes 6148
  224.4 219.9 %copy-start.13 = (f32[512]{0:T(512)S(1)}, f32[512]{0:T(512)}, u32[]{:S(2)}) copy-start(f32[512]{0:T(512)} %param.40) | copy-start | bytes 6148
Sparse Core Ops, SparseCore 0:
  9.5 43.0 all-gather.5
  75.3 23.6 reduce-scatter.2
  107.9 17.3 all-gather.7
  127.3 92.2 all-gather.9
  221.6 90.4 all-gather.11
  314.0 91.2 all-gather.13
  414.4 22.9 reduce-scatter.4
where the time goes:
time: 454 us; the launch traced here: 453 us
  waiting for transfers between devices  348 us (77%)
  blocking collectives  44.4 us (10%)
  matrix products  33.3 us (7%)
  between operations  13.7 us (3%)
  other arithmetic  10.3 us (2%)
    all_gather x1, waiting for transfers between devices, body(): lax.all_gather(gate_weight, 'sp', axis=0, tiled=True)  94.4 us
    all_gather x1, waiting for transfers between devices, body(): lax.all_gather(down_weight, 'sp', axis=1, tiled=True)  93.2 us
    all_gather x1, waiting for transfers between devices, body(): lax.all_gather(up_weight, 'sp', axis=0, tiled=True)  87.8 us
    all_gather x1, blocking collectives, body(): lax.all_gather(rotary_key, 'sp', axis=0, tiled=True)  32.8 us
    reduce_scatter x1, waiting for transfers between devices, body(): lax.psum_scatter(terms.astype(jnp.bfloat16), 'tp', scatter_dimension=1, t...  23.7 us
    reduce_scatter x1, waiting for transfers between devices, body(): lax.psum_scatter(feed_terms.astype(jnp.bfloat16), 'tp', scatter_dimension...  23.1 us
    all_gather x1, waiting for transfers between devices, body(): full_rows = lax.all_gather(normed_first, 'tp', axis=1, tiled=True)  15.5 us
  transfers between devices with their start and end apart: 7, of which 7 were waited for; matrix products, arithmetic and copies ran while one was open for 2% of the time, Pallas kernels for 0%

commit v1 on v0

--- a/solution.py
+++ b/solution.py
@@ -179,7 +179,7 @@
     hidden = (jax.nn.silu(gate_part) * lifted_part).astype(jnp.bfloat16)
     feed_terms = jnp.dot(
         hidden,
-        lax.all_gather(down_weight, "sp", axis=1, tiled=True),
+        jnp.concatenate(lax.all_gather(down_weight, "sp"), axis=1),
         preferred_element_type=jnp.float32,
     )
     feed = lax.psum_scatter(

time: 454 us -> 446 us (0.982)
  waiting for transfers between devices: 348 us -> 331 us
  local copies, waits for them, and re-layouts: 2.91 us -> 9.71 us
    all_gather x1, waiting for transfers between devices: 93.2 us -> 84.3 us  [body(): lax.all_gather(down_weight, 'sp')]
    reshape x0 -> x1, local copies, waits for them, and re-layouts: none -> 8.33 us  [body(): jnp.concatenate(lax.all_gather(down_weight, 'sp'), axis=1)]
    all_gather x1, waiting for transfers between devices: 15.5 us -> 8.01 us  [body(): full_rows = lax.all_gather(normed_first, 'tp', axis=1, tiled=True)]
  transfers between devices with their start and end apart: 7 -> 7, of which waited for: 7 -> 7; matrix products, arithmetic and copies ran while one was open for 2% -> 5% of each run, Pallas kernels for 0% -> 0%
where the time goes in v1:
time: 446 us; the launch traced here: 445 us
  waiting for transfers between devices  331 us (74%)
  blocking collectives  44.4 us (10%)
  matrix products  34.4 us (8%)
  between operations  13.7 us (3%)
  other arithmetic  12 us (3%)
  local copies, waits for them, and re-layouts  9.71 us (2%)
    all_gather x1, waiting for transfers between devices, body(): lax.all_gather(gate_weight, 'sp', axis=0, tiled=True)  94.4 us
    all_gather x1, waiting for transfers between devices, body(): lax.all_gather(up_weight, 'sp', axis=0, tiled=True)  87.8 us
    all_gather x1, waiting for transfers between devices, body(): lax.all_gather(down_weight, 'sp')  84.3 us
    all_gather x1, blocking collectives, body(): lax.all_gather(rotary_key, 'sp', axis=0, tiled=True)  32.8 us
    reduce_scatter x1, waiting for transfers between devices, body(): lax.psum_scatter(feed_terms.astype(jnp.bfloat16), 'tp', scatter_dimension...  23.2 us
    reduce_scatter x1, waiting for transfers between devices, body(): lax.psum_scatter(terms.astype(jnp.bfloat16), 'tp', scatter_dimension=1, t...  23 us
  transfers between devices with their start and end apart: 7, of which 7 were waited for; matrix products, arithmetic and copies ran while one was open for 5% of the time, Pallas kernels for 0%

profile of v1, /device:TPU:0, one launch (start us, length us, event | category | flops | bytes accessed | tf_op | source)
XLA Modules:
  0.0 445.1 jit_solution(17800248615906493966)
XLA Ops:
  6.5 0.7 all-gather.7.cloned.1.call-update
  7.4 32.8 %all_gather.22 = bf16[2048,32]{0,1:T(8,128)(2,1)S(1)} all-gather(bf16[256,32]{0,1:T(8,128)(2,1)} %param.24), channel_id=1, replica_groups=mesh['sp'=8,'tp'=4] {'sp'}, dimensions={0}, use_global_device_ids=true | all-gather | bytes 147456 | tf_op jit(solution)/shard_map/all_gather | solution.py:127
  40.2 1.1 fusion.31
  41.3 1.3 convolution_bitcast_fusion.5
  42.6 1.3 convolution_bitcast_fusion.4
  45.2 7.4 %all-gather.7.cloned.1.call-done = bf16[2048,256]{1,0:T(8,128)(2,1)} async-done(((bf16[256,256]{1,0:T(8,128)(2,1)}), bf16[2048,256]{1,0:T(8,128)(2,1)}) %all-gather.7.cloned.1.call-update) | async-done | bytes 1048592 | tf_op jit(solution)/shard_map/all_gather | solution.py:126
  52.5 1.6 fusion.6
  54.2 3.4 fusion.132
  57.5 2.1 fusion.9
  59.7 2.2 convolution_bitcast_fusion.1
  61.9 2.1 fusion.131
  64.1 1.3 copy-done.2
  65.8 2.6 fusion.22
  68.5 1.8 fusion.135
  70.2 2.5 fusion.24
  72.8 3.1 fusion.4
  76.0 0.7 all-gather.15.cloned.1.call-update
  76.7 23.0 %reduce-scatter.3.cloned.1.call-done = bf16[256,512]{1,0:T(8,128)(2,1)} async-done(((bf16[256,2048]{1,0:T(8,128)(2,1)}), bf16[256,512]{1,0:T(8,128)(2,1)}) %reduce-scatter.3.cloned.1.call-update) | async-done | bytes 262160 | tf_op jit(solution)/shard_map/reduce_scatter | solution.py:165
  99.7 1.2 fusion.34
  100.9 5.8 %all-reduce.1 = (f32[256]{0:T(256)S(1)}, f32[256]{0:T(256)S(1)}) all-reduce(f32[256]{0:T(256)S(1)} %get-tuple-element.8, f32[256]{0:T(256)S(1)} %get-tuple-element.7), channel_id=1, replica_groups=mesh['sp'=8,'tp'=4] {'tp'}, use_global_device_ids=true, to_apply=%region_10.11 | all-reduce | flops 512 | bytes 4096 | tf_op jit(solution)/shard_map/psum | solution.py:170
  106.6 1.8 add_convert_fusion.1
  109.9 84.3 %all-gather.15.cloned.1.call-done = bf16[11264,256]{1,0:T(8,128)(2,1)} async-done(((bf16[1408,256]{1,0:T(8,128)(2,1)}), bf16[11264,256]{1,0:T(8,128)(2,1)}) %all-gather.15.cloned.1.call-update) | async-done | bytes 5767184 | tf_op jit(solution)/shard_map/all_gather | solution.py:182
  194.2 8.3 %copy.28 = bf16[1408,8,256]{0,2,1:T(8,128)(2,1)} copy(bf16[1408,8,256]{2,0,1:T(8,128)(2,1)} %bitcast.104) | data formatting | bytes 11534336 | tf_op jit(solution)/shard_map/reshape | solution.py:182
  202.5 8.0 %all-gather.9.cloned.1.call-done = bf16[256,2048]{1,0:T(8,128)(2,1)} async-done(((bf16[256,512]{1,0:T(8,128)(2,1)}), bf16[256,2048]{1,0:T(8,128)(2,1)}) %all-gather.9.cloned.1.call-update) | async-done | bytes 1048592 | tf_op jit(solution)/shard_map/all_gather | solution.py:172
  210.6 94.4 %all-gather.11.cloned.1.call-done = bf16[2048,1408]{1,0:T(8,128)(2,1)} async-done(((bf16[256,1408]{1,0:T(8,128)(2,1)}), bf16[2048,1408]{1,0:T(8,128)(2,1)}) %all-gather.11.cloned.1.call-update) | async-done | bytes 5767184 | tf_op jit(solution)/shard_map/all_gather | solution.py:174
  304.9 4.8 %fusion.136 = f32[256,1408]{1,0:T(8,128)S(1)} fusion(bf16[256,2048]{1,0:T(8,128)(2,1)} %all-gather.9.cloned.1.call-done, bf16[2048,1408]{1,0:T(8,128)(2,1)} %all-gather.11.cloned.1.call-done), kind=kOutput, calls=%fused_computation.179 | convolution fusion | flops 1476395008 | bytes 8257536 | tf_op jit(solution)/shard_map/dot_general | solution.py:177
  309.7 87.8 %all-gather.13.cloned.1.call-done = bf16[2048,1408]{1,0:T(8,128)(2,1)} async-done(((bf16[256,1408]{1,0:T(8,128)(2,1)}), bf16[2048,1408]{1,0:T(8,128)(2,1)}) %all-gather.13.cloned.1.call-update) | async-done | bytes 5767184 | tf_op jit(solution)/shard_map/all_gather | solution.py:175
  397.5 8.8 %convolution_convert_fusion = bf16[256,2048]{1,0:T(8,128)(2,1)} fusion(bf16[1408,2048]{0,1:T(8,128)(2,1)} %bitcast.105, bf16[256,2048]{1,0:T(8,128)(2,1)S(1)} %copy-done.13, bf16[2048,1408]{1,0:T(8,128)(2,1)} %all-gather.13.cloned.1.call-done, f32[256,1408]{1,0:T(8,128)S(1)} %fusion.136), kind=kOutput, calls=%fused_computation.14 | convolution fusion | flops 2955476992 | bytes 15073280 | tf_op jit(solution)/shard_map/dot_general | solution.py:180
  406.3 23.2 %reduce-scatter.5.cloned.1.call-done = bf16[256,512]{1,0:T(8,128)(2,1)} async-done(((bf16[256,2048]{1,0:T(8,128)(2,1)}), bf16[256,512]{1,0:T(8,128)(2,1)}) %reduce-scatter.5.cloned.1.call-update) | async-done | bytes 262160 | tf_op jit(solution)/shard_map/reduce_scatter | solution.py:185
  429.5 1.2 fusion.35
  430.6 5.8 %all-reduce = (f32[256]{0:T(256)S(1)}, f32[256]{0:T(256)S(1)}) all-reduce(f32[256]{0:T(256)S(1)} %get-tuple-element.6, f32[256]{0:T(256)S(1)} %get-tuple-element.5), channel_id=1, replica_groups=mesh['sp'=8,'tp'=4] {'tp'}, use_global_device_ids=true, to_apply=%region_15.16 | all-reduce | flops 512 | bytes 4096 | tf_op jit(solution)/shard_map/psum | solution.py:189
  436.4 1.8 add_convert_fusion
  (57 shorter events, 3.3 us)
Async XLA Ops:
  6.5 61.9 %copy-start = (bf16[128,2048]{1,0:T(8,128)(2,1)S(1)}, bf16[128,2048]{1,0:T(8,128)(2,1)}, u32[]{:S(2)}) copy-start(bf16[128,2048]{1,0:T(8,128)(2,1)} %param.34) | copy-start | bytes 1572868
  6.5 46.0 %all-gather.7.cloned.1.call-start = ((), (), s32[]{:S(2)}) async-start(), calls=%async_computation.2 | async-start | bytes 1179648 | tf_op jit(solution)/shard_map/all_gather | solution.py:126
  7.3 92.4 %reduce-scatter.3.cloned.1.call-start = ((), (), s32[]{:S(2)}) async-start(), calls=%async_computation.3 | async-start | bytes 1310720 | tf_op jit(solution)/shard_map/reduce_scatter | solution.py:165
  43.9 10.2 %copy-start.7 = (bf16[256,64]{0,1:T(8,128)(2,1)S(1)}, bf16[256,64]{0,1:T(8,128)(2,1)}, u32[]{:S(2)}) copy-start(bf16[256,64]{0,1:T(8,128)(2,1)} %param.28) | copy-start | bytes 98308
  43.9 10.2 %copy-start.8 = (f32[256]{0:T(256)S(1)}, f32[256]{0:T(256)}, u32[]{:S(2)}) copy-start(f32[256]{0:T(256)} %param.26) | copy-start | bytes 3076
  57.5 2.1 copy-start.1
  57.5 2.1 copy-start.6
  64.1 1.3 copy-start.2
  64.1 1.8 copy-start.14
  68.5 1.8 copy-start.15
  70.2 2.5 copy-start.5
  72.8 26.9 %copy-start.4 = (bf16[256,512]{1,0:T(8,128)(2,1)S(1)}, bf16[256,512]{1,0:T(8,128)(2,1)}, u32[]{:S(2)}) copy-start(bf16[256,512]{1,0:T(8,128)(2,1)} %param.21) | copy-start | bytes 786436
  72.8 33.8 %copy-start.9 = (f32[512]{0:T(512)S(1)}, f32[512]{0:T(512)}, u32[]{:S(2)}) copy-start(f32[512]{0:T(512)} %param.36) | copy-start | bytes 6148
  72.8 33.8 %copy-start.10 = (f32[512]{0:T(512)S(1)}, f32[512]{0:T(512)}, u32[]{:S(2)}) copy-start(f32[512]{0:T(512)} %param.35) | copy-start | bytes 6148
  75.9 118.3 %all-gather.15.cloned.1.call-start = ((), (), s32[]{:S(2)}) async-start(), calls=%async_computation.8 | async-start | bytes 6488064 | tf_op jit(solution)/shard_map/all_gather | solution.py:182
  76.7 133.9 %all-gather.9.cloned.1.call-start = ((), (), s32[]{:S(2)}) async-start(), calls=%async_computation.4 | async-start | bytes 1310720 | tf_op jit(solution)/shard_map/all_gather | solution.py:172
  108.5 196.4 %all-gather.11.cloned.1.call-start = ((), (), s32[]{:S(2)}) async-start(), calls=%async_computation.5 | async-start | bytes 6488064 | tf_op jit(solution)/shard_map/all_gather | solution.py:174
  109.1 288.4 %all-gather.13.cloned.1.call-start = ((), (), s32[]{:S(2)}) async-start(), calls=%async_computation.6 | async-start | bytes 6488064 | tf_op jit(solution)/shard_map/all_gather | solution.py:175
  109.7 319.8 %reduce-scatter.5.cloned.1.call-start = ((), (), s32[]{:S(2)}) async-start(), calls=%async_computation.7 | async-start | bytes 1310720 | tf_op jit(solution)/shard_map/reduce_scatter | solution.py:185
  210.6 186.9 %copy-start.13 = (bf16[256,2048]{1,0:T(8,128)(2,1)S(1)}, bf16[256,2048]{1,0:T(8,128)(2,1)}, u32[]{:S(2)}) copy-start(bf16[256,2048]{1,0:T(8,128)(2,1)} %all-gather.9.cloned.1.call-done) | copy-start | bytes 3145732
  397.5 32.0 %copy-start.3 = (bf16[256,512]{1,0:T(8,128)(2,1)S(1)}, bf16[256,512]{1,0:T(8,128)(2,1)}, u32[]{:S(2)}) copy-start(bf16[256,512]{1,0:T(8,128)(2,1)} %add_convert_fusion.1) | copy-start | bytes 786436
  397.5 38.9 %copy-start.11 = (f32[512]{0:T(512)S(1)}, f32[512]{0:T(512)}, u32[]{:S(2)}) copy-start(f32[512]{0:T(512)} %param.41) | copy-start | bytes 6148
  397.5 38.9 %copy-start.12 = (f32[512]{0:T(512)S(1)}, f32[512]{0:T(512)}, u32[]{:S(2)}) copy-start(f32[512]{0:T(512)} %param.40) | copy-start | bytes 6148
Sparse Core Ops, SparseCore 0:
  9.5 43.0 all-gather.6
  76.1 23.6 reduce-scatter.2
  101.9 92.2 all-gather.14
  195.6 14.8 all-gather.8
  212.6 92.2 all-gather.10
  307.0 90.4 all-gather.12
  406.4 22.9 reduce-scatter.4
